TPU v7x, 32 devices: a whole 2x2x4 slice. The times are simulated.
32 devices in a mesh: gr: 2 (over x), sp: 8 (over z, y), tp: 2 (over core).
Axes of the slice: x: 2, y: 2, z: 4, core: 2. Of those that a mesh axis runs over, the one named last changes fastest.
Arguments:
- prompt: bfloat16 [2, 2048, 4096], P('gr', 'sp', 'tp'), parts along dimension 0, may hold values from -6 to 6
- key_weight: bfloat16 [4096, 4096], P(None, 'tp'), may hold values from -0.09375 to 0.09375
- value_weight: bfloat16 [4096, 4096], P(None, 'tp'), may hold values from -0.375 to 0.375
- beta_weight: bfloat16 [4096, 32], P(None, 'tp'), may hold values from -0.09375 to 0.09375
- beta_bias: float32 [32], P('tp'), may hold values from -4.5 to -0.5
- decay_rate: float32 [32], P('tp'), may hold values from 0.1 to 3
- new_query: bfloat16 [2, 32, 128], P('gr', 'tp'), parts along dimension 0, may hold values from -6 to 6
- read_gain: float32 [128], replicated, may hold values from 0.1 to 1.9
Outputs:
- state_cache: bfloat16 [2, 32, 128, 128], P('gr', 'tp', 'sp'), parts along dimension 0
- first_read: float32 [2, 32, 128], P('gr', 'tp'), parts along dimension 0
There are 2 independent parts, one for each index of `gr`. A program takes and returns all parts, laid end to end along the dimension named above; an argument that names none is the same for every part. Nothing has to cross between parts.
All inputs are finite; a program needn't handle non-finite values.
Results may differ from a plain program's by a relative error of at most 0.013.
Values may be sent and summed in bfloat16 or wider, within the bound.
A program may use at most 128 MiB of HBM per device.

v0:
```python
import functools

import jax
import jax.numpy as jnp
from jax import lax
from jax.experimental import pallas as pl
from jax.experimental.pallas import tpu as pltpu
from jax.sharding import PartitionSpec as P

MESH = pl.DeviceIdType.MESH
F32 = jnp.float32
BF16 = jnp.bfloat16


def dot(left, right, contract=((1,), (0,))):
    return lax.dot_general(left, right, (contract, ((), ())), preferred_element_type=F32)


def level_masks(size):
    row = lax.broadcasted_iota(jnp.int32, (size, size), 0)
    col = lax.broadcasted_iota(jnp.int32, (size, size), 1)
    masks = []
    for level in range((size - 1).bit_length()):
        together = (row >> (level + 1)) == (col >> (level + 1))
        apart = (row >> level) != (col >> level)
        masks.append((together & apart & (row > col)).astype(F32).astype(BF16))
    return masks


def span(heads, masks, eye):
    keys_t, rights, grams, inverses = [], [], [], []
    for key, value, strength, fade in heads:
        key = key.astype(F32)
        key = key * lax.rsqrt(jnp.sum(key * key, axis=1, keepdims=True) + 1.0)
        weighted = (key * strength).astype(BF16)
        key = key.astype(BF16)
        value = (value.astype(F32) * (strength * fade)).astype(BF16)
        keys_t.append(key)
        rights.append(jnp.concatenate([value, weighted], axis=1))
        grams.append(dot(weighted, key, ((1,), (1,))).astype(BF16))
    for gram in grams:
        inverses.append(eye[...] - gram * masks[0])
    size = grams[0].shape[0]
    levels = (size - 1).bit_length()
    for level in range(1, levels - 1):
        steps = [dot(g * masks[level], x).astype(BF16) for g, x in zip(grams, inverses)]
        inverses = [x - dot(x, s).astype(BF16) for x, s in zip(inverses, steps)]
    half = size // 2
    out = []
    for key, right, gram, x in zip(keys_t, rights, grams, inverses):
        first, last = x[:half, :half], x[half:, half:]
        cross = dot(last, dot(gram[half:, :half], first).astype(BF16)).astype(BF16)
        top, low = key[:half], key[half:]
        y_first = dot(top, first, ((0,), (0,))) - dot(low, cross, ((0,), (0,)))
        y_last = dot(low, last, ((0,), (0,)))
        y = jnp.concatenate([y_first.astype(BF16), y_last.astype(BF16)], axis=1)
        out.append(dot(y, right))
    return out


def kernel(
    n, tp, groups, per, dim, together,
    prompt, key_w, value_w, beta_w, bias, decay, query, gain,
    state_out, read_out,
    feat, first_buf, rest_buf, total, beta_buf, bias_buf, decay_buf, query_buf, gain_buf,
    mask_buf, eye_buf, strength_buf, spans, partner_spans, joined, recv,
    row_stage, row_recv, read_stage, read_recv,
    in_sem, feat_send, feat_recv, first_sem, rest_sem, pair_send, pair_recv,
    map_send, map_recv, row_send, row_got, read_send, read_got,
):
    me = lax.axis_index("sp")
    core = lax.axis_index("tp")
    seg, part = prompt.shape[1], prompt.shape[2]
    wide = per * dim
    full = seg * n
    stride = n // groups
    half = groups // 2
    parity = lax.rem(me, 2)
    mine = me // stride
    slots = first_buf.shape[0]

    def owner(g):
        return g * stride + (lax.rem(g, 2) if stride > 1 else 0)

    is_owner = me == owner(mine)

    def when_owner(work):
        if stride == 1:
            work()
        else:
            pl.when(is_owner)(work)

    def pair_at(j):
        return lax.rem(mine // 2 + 1 + j, half)

    def place(index):
        step, s = index // together, lax.rem(index, together)
        return lax.rem(step, 2), pair_at(step // 2 * together + s)

    def group_at(index):
        keep, m = place(index)
        return 2 * m + keep * parity + (1 - keep) * (1 - parity)

    def columns(g):
        return pl.ds(pl.multiple_of(g * wide, wide), wide)

    def features_of(d):
        return pl.ds(pl.multiple_of(lax.rem(core + d, tp) * part, part), part)

    def fetch_first(index):
        slot = lax.rem(index, slots)
        return [
            pltpu.make_async_copy(
                w.at[features_of(0), columns(group_at(index))], first_buf.at[slot, j], first_sem.at[slot, j]
            )
            for j, w in enumerate((key_w, value_w))
        ]

    def fetch_rest(step):
        slot = lax.rem(step, 2)
        return [
            pltpu.make_async_copy(
                w.at[features_of(d), columns(group_at(step * together + s))],
                rest_buf.at[slot, s, j, d - 1], rest_sem.at[slot, s, j, d - 1],
            )
            for s in range(together)
            for j, w in enumerate((key_w, value_w))
            for d in range(1, tp)
        ]

    own_prompt = pltpu.make_async_copy(prompt.at[0], feat.at[core], in_sem.at[0])
    small = [
        pltpu.make_async_copy(src, dst, in_sem.at[1 + k])
        for k, (src, dst) in enumerate(
            ((beta_w, beta_buf), (bias, bias_buf), (decay, decay_buf), (query, query_buf), (gain, gain_buf))
        )
    ]
    own_prompt.start()
    for index in range(min(slots - 1, groups)):
        for copy in fetch_first(index):
            copy.start()
    for copy in small:
        copy.start()

    barrier = pltpu.get_barrier_semaphore()
    for d in range(1, n):
        pl.semaphore_signal(barrier, inc=1, device_id={"sp": lax.rem(me + d, n)}, device_id_type=MESH)
    for d in range(1, tp):
        pl.semaphore_signal(barrier, inc=1, device_id={"tp": lax.rem(core + d, tp)}, device_id_type=MESH)
    own_prompt.wait()
    pl.semaphore_wait(barrier, n - 1 + tp - 1)

    def feature_copy(d, slot):
        return pltpu.make_async_remote_copy(
            src_ref=feat.at[core], dst_ref=feat.at[slot],
            send_sem=feat_send.at[d - 1], recv_sem=feat_recv.at[slot],
            device_id={"tp": lax.rem(core + d, tp)}, device_id_type=MESH,
        )

    for d in range(1, tp):
        feature_copy(d, core).start()

    def project_first(index, carry):
        @pl.when(index + slots - 1 < groups)
        def _():
            for copy in fetch_first(index + slots - 1):
                copy.start()

        for copy in fetch_first(index):
            copy.wait()
        slot, g = lax.rem(index, slots), group_at(index)
        for j in range(2):
            total[g, j] = dot(feat[core], first_buf[slot, j])
        return carry

    lax.fori_loop(0, groups, project_first, 0)
    for copy in fetch_rest(0):
        copy.start()

    for level, mask in enumerate(level_masks(seg)):
        mask_buf[level] = mask
    ids = [lax.broadcasted_iota(jnp.int32, (seg, seg), axis) for axis in (0, 1)]
    eye_buf[...] = (ids[0] == ids[1]).astype(F32).astype(BF16)
    for copy in small:
        copy.wait()
    before = dot(feat[core], beta_buf[:, features_of(0)], ((1,), (1,)))
    for d in range(1, tp):
        other = lax.rem(core + d, tp)
        feature_copy(d, other).wait_recv()
        before += dot(feat[other], beta_buf[:, features_of(d)], ((1,), (1,)))
    strength_buf[...] = jax.nn.sigmoid(before + bias_buf[...])

    def pair_copy(m):
        return pltpu.make_async_remote_copy(
            src_ref=spans.at[0, m], dst_ref=partner_spans.at[m],
            send_sem=pair_send.at[m], recv_sem=pair_recv.at[m],
            device_id={"sp": me + 1 - 2 * parity}, device_id_type=MESH,
        )

    def map_copy(m, slot):
        return pltpu.make_async_remote_copy(
            src_ref=joined.at[m], dst_ref=recv.at[slot],
            send_sem=map_send.at[m], recv_sem=map_recv.at[slot],
            device_id={"sp": owner(2 * m + parity)}, device_id_type=MESH,
        )

    def send(step):
        for s in range(together):
            keep, m = place(step * together + s)

            @pl.when(keep == 0)
            def _():
                pair_copy(m).start()

            @pl.when((keep == 1) & (owner(2 * m + parity) != me))
            def _():
                map_copy(m, me // 2).start()

    def body(step, carry):
        slot = lax.rem(step, 2)

        @pl.when(step + 1 < groups // together)
        def _():
            for copy in fetch_rest(step + 1):
                copy.start()

        @pl.when(step > 0)
        def _():
            send(step - 1)

        for copy in fetch_rest(step):
            copy.wait()
        projected = []
        for s in range(together):
            g = group_at(step * together + s)
            pair = []
            for j in range(2):
                acc = total[g, j]
                for d in range(1, tp):
                    acc += dot(feat[lax.rem(core + d, tp)], rest_buf[slot, s, j, d - 1])
                pair.append(acc.astype(BF16))
            projected.append(pair)

        strengths = strength_buf[...]
        rates = decay_buf[...]
        lane = lax.broadcasted_iota(jnp.int32, strengths.shape, 1)
        rest = full - 1 - me * seg - lax.broadcasted_iota(jnp.int32, (seg, 1), 0)
        rest = rest.astype(F32) * (1.0 / full)
        heads = []
        for s in range(together):
            g = group_at(step * together + s)
            keys, values = projected[s]
            for h in range(per):
                head = g * per + h
                strength = jnp.sum(jnp.where(lane == head, strengths, 0.0), axis=1, keepdims=True)
                rate = jnp.sum(jnp.where(lane[:1] == head, rates, 0.0), axis=1, keepdims=True)
                fade = jnp.exp(-rate * rest)
                cols = slice(h * dim, (h + 1) * dim)
                heads.append((keys[:, cols], values[:, cols], strength, fade))
        keep = lax.rem(step, 2)
        for k, result in enumerate(span(heads, mask_buf, eye_buf)):
            m = place(step * together + k // per)[1]
            spans[keep, m, k % per] = result.astype(BF16)

        @pl.when(keep == 1)
        def _():
            for s in range(together):
                m = place(step * together + s)[1]
                pair_copy(m).wait_recv()
                for h in range(per):
                    ours, theirs = spans[1, m, h], partner_spans[m, h]
                    early = jnp.where(parity == 1, theirs, ours)
                    late = jnp.where(parity == 1, ours, theirs)
                    both = early.astype(F32) + late.astype(F32) - dot(late[:, dim:], early)
                    joined[m, h] = both.astype(BF16)

        return carry

    lax.fori_loop(0, groups // together, body, 0)
    recv[me // 2] = joined[mine // 2]
    send(groups // together - 1)

    rows = dim // n

    def row_copy(q, slot):
        return pltpu.make_async_remote_copy(
            src_ref=row_stage.at[q], dst_ref=row_recv.at[slot],
            send_sem=row_send.at[q], recv_sem=row_got.at[slot],
            device_id={"sp": q}, device_id_type=MESH,
        )

    def read_copy(q, slot):
        return pltpu.make_async_remote_copy(
            src_ref=read_stage, dst_ref=read_recv.at[slot],
            send_sem=read_send.at[q], recv_sem=read_got.at[slot],
            device_id={"sp": q}, device_id_type=MESH,
        )

    def finish():
        def link(p, states):
            @pl.when(p != me // 2)
            def _():
                map_copy(0, p).wait_recv()

            new = []
            for h in range(per):
                write, drop = recv[p, h, :, :dim].astype(F32), recv[p, h, :, dim:]
                high = states[h].astype(BF16)
                low = (states[h] - high.astype(F32)).astype(BF16)
                new.append(states[h] + (write - dot(drop, high) - dot(drop, low)))
            return tuple(new)

        states = lax.fori_loop(0, n // 2, link, tuple(jnp.zeros((dim, dim), F32) for _ in range(per)))
        for h in range(per):
            cast = states[h].astype(BF16)
            for q in range(n):
                row_stage[q, h] = cast[q * rows:(q + 1) * rows]
        unit = query_buf[0].astype(F32)
        unit = unit * lax.rsqrt(jnp.sum(unit * unit, axis=1, keepdims=True) + 1.0)
        which = lax.broadcasted_iota(jnp.int32, unit.shape, 0)
        for h in range(per):
            row = jnp.sum(jnp.where(which == mine * per + h, unit, 0.0), axis=0, keepdims=True)
            raw = jnp.dot(
                jnp.broadcast_to(row, (8, dim)), states[h],
                precision=lax.Precision.HIGHEST, preferred_element_type=F32,
            )[0:1]
            raw = raw * lax.rsqrt(jnp.mean(raw * raw, axis=1, keepdims=True) + 0.05) * gain_buf[...]
            read_stage[h:h + 1] = raw
        for d in range(1, n):
            row_copy(lax.rem(me + d, n), mine).start()
        for d in range(1, n):
            read_copy(lax.rem(me + d, n), mine).start()
        row_recv[mine] = row_stage[me]
        read_recv[mine] = read_stage[...]

    when_owner(finish)

    for g in range(groups):
        @pl.when(me != owner(g))
        def _():
            row_copy(me, g).wait_recv()
            read_copy(me, g).wait_recv()

        for h in range(per):
            state_out[0, g * per + h] = row_recv[g, h]
        read_out[0, g * per:(g + 1) * per] = read_recv[g]

    for d in range(1, tp):
        feature_copy(d, core).wait_send()
    for m in range(half):
        pair_copy(m).wait_send()

        @pl.when(owner(2 * m + parity) != me)
        def _():
            map_copy(m, 0).wait_send()

    def sent():
        for d in range(1, n):
            row_copy(lax.rem(me + d, n), mine).wait_send()
            read_copy(lax.rem(me + d, n), mine).wait_send()

    when_owner(sent)


def solution(mesh):
    n, tp = mesh.shape["sp"], mesh.shape["tp"]

    def shards(prompt, key_w, value_w, beta_w, bias, decay, query, gain):
        seg, part = prompt.shape[1:]
        depth = key_w.shape[0]
        heads = beta_w.shape[1]
        dim = key_w.shape[1] // heads
        per = max(1, heads // n)
        groups = heads // per
        wide = per * dim
        rows = dim // n
        levels = (seg - 1).bit_length()
        dma = pltpu.SemaphoreType.DMA
        vmem = pl.BlockSpec(memory_space=pltpu.VMEM)
        hbm = pl.BlockSpec(memory_space=pl.ANY)
        half = groups // 2
        together = min(2, half)
        slots = 4
        return pl.pallas_call(
            functools.partial(kernel, n, tp, groups, per, dim, together),
            out_shape=(
                jax.ShapeDtypeStruct((1, heads, rows, dim), BF16),
                jax.ShapeDtypeStruct((1, heads, dim), F32),
            ),
            in_specs=[hbm] * 8,
            out_specs=(vmem, vmem),
            scratch_shapes=[
                pltpu.VMEM((tp, seg, part), BF16),
                pltpu.VMEM((slots, 2, part, wide), BF16),
                pltpu.VMEM((2, together, 2, tp - 1, part, wide), BF16),
                pltpu.VMEM((groups, 2, seg, wide), F32),
                pltpu.VMEM((heads, depth), BF16),
                pltpu.VMEM((1, heads), F32),
                pltpu.VMEM((1, heads), F32),
                pltpu.VMEM((1, heads, dim), BF16),
                pltpu.VMEM((1, dim), F32),
                pltpu.VMEM((levels, seg, seg), BF16),
                pltpu.VMEM((seg, seg), BF16),
                pltpu.VMEM((seg, heads), F32),
                pltpu.VMEM((2, half, per, dim, 2 * dim), BF16),
                pltpu.VMEM((half, per, dim, 2 * dim), BF16),
                pltpu.VMEM((half, per, dim, 2 * dim), BF16),
                pltpu.VMEM((n // 2, per, dim, 2 * dim), BF16),
                pltpu.VMEM((n, per, rows, dim), BF16),
                pltpu.VMEM((groups, per, rows, dim), BF16),
                pltpu.VMEM((per, dim), F32),
                pltpu.VMEM((groups, per, dim), F32),
                dma((6,)),
                dma((tp - 1,)),
                dma((tp,)),
                dma((slots, 2)),
                dma((2, together, 2, tp - 1)),
                dma((half,)),
                dma((half,)),
                dma((half,)),
                dma((n // 2,)),
                dma((n,)),
                dma((groups,)),
                dma((n,)),
                dma((groups,)),
            ],
            compiler_params=pltpu.CompilerParams(
                collective_id=0, has_side_effects=True, vmem_limit_bytes=60 * 2**20
            ),
        )(
            prompt, key_w, value_w, beta_w.T, bias.reshape(1, heads), decay.reshape(1, heads),
            query, gain.reshape(1, dim),
        )

    return jax.shard_map(
        shards,
        mesh=mesh,
        in_specs=(
            P("gr", "sp", "tp"),
            P(None, "tp"),
            P(None, "tp"),
            P(None, "tp"),
            P("tp"),
            P("tp"),
            P("gr", "tp", None),
            P(),
        ),
        out_specs=(P("gr", "tp", "sp", None), P("gr", "tp", None)),
        check_vma=False,
    )
```

profile of v0, /device:TPU:0, one launch (start us, length us, event | category | flops | bytes accessed | tf_op | source)
XLA Modules:
  0.0 52.5 jit_solution(13483135314135364557)
XLA Ops:
  0.6 49.1 %shard_map.95 = (bf16[1,16,16,128]{3,2,1,0:T(8,128)(2,1)}, f32[1,16,128]{2,1,0:T(8,128)}) custom-call(bf16[1,256,2048]{2,1,0:T(8,128)(2,1)} %prompt.1, bf16[4096,2048]{1,0:T(8,128)(2,1)} %key_w.1, bf16[4096,2048]{1,0:T(8,128)(2,1)} %value_w.1, bf16[16,4096]{1,0:T(8,128)(2,1)} %bitcast.4, f32[1,16]{1,0:T(1,128)} %bitcast.5, f32[1,16]{1,0:T(1,128)} %bitcast.6, ...), custom_call_target="tpu_custom_call" | custom-call | tf_op jit(solution)/shard_map/pallas_call | solution.py:384
  49.8 1.5 %copy.12 = bf16[1,16,16,128]{3,2,1,0:T(8,128)(2,1)} copy(bf16[1,16,16,128]{3,2,1,0:T(8,128)(2,1)} %get-tuple-element.4) | data formatting | bytes 131072
  51.2 1.3 %copy.13 = f32[1,16,128]{2,1,0:T(8,128)} copy(f32[1,16,128]{2,1,0:T(8,128)} %get-tuple-element.5) | data formatting | bytes 16384
where the time goes:
time: 52.8 us; the launch traced here: 52.5 us
  Pallas kernels  49.1 us (93%)
  local copies, waits for them, and re-layouts  2.77 us (5%)
  between operations  0.64 us (1%)
    pallas_call x1, Pallas kernels, shards(): pl.pallas_call(functools.partial(kernel, n, tp, groups, per, dim, togethe...  49.1 us
    unnamed x2, local copies, waits for them, and re-layouts  2.77 us

commit v1 on v0

v1 whole, which is shorter than its diff:
```python
import functools

import jax
import jax.numpy as jnp
from jax import lax
from jax.experimental import pallas as pl
from jax.experimental.pallas import tpu as pltpu
from jax.sharding import PartitionSpec as P

MESH = pl.DeviceIdType.MESH
F32 = jnp.float32
BF16 = jnp.bfloat16


def dot(left, right, contract=((1,), (0,))):
    return lax.dot_general(left, right, (contract, ((), ())), preferred_element_type=F32)


def bounds(size):
    levels = (size - 1).bit_length()
    cuts = [0, min(3, levels)]
    while cuts[-1] < levels:
        cuts.append(min(cuts[-1] + 2, levels))
    return tuple(zip(cuts[:-1], cuts[1:]))


def cut_masks(size):
    row = lax.broadcasted_iota(jnp.int32, (size, 2 * size), 0)
    col = lax.rem(lax.broadcasted_iota(jnp.int32, (size, 2 * size), 1), size)
    masks = []
    for low, high in bounds(size):
        together = (row >> high) == (col >> high)
        apart = (row >> low) != (col >> low)
        masks.append((together & apart & (row > col)).astype(F32).astype(BF16))
    return masks, (row == col).astype(F32).astype(BF16)


def spread(x):
    size = x.shape[1] // 2
    zero = jnp.zeros((x.shape[0], size), x.dtype)
    return jnp.concatenate(
        [jnp.concatenate([x[:, :size], zero], axis=1), jnp.concatenate([zero, x[:, size:]], axis=1)], axis=0
    )


def under(x, y):
    return jnp.concatenate([x, y], axis=0)


def mul(x, y):
    return dot(x, spread(y)).astype(BF16)


def span(heads, masks, eye, tick):
    keys_t, rights, grams = [], [], []
    for key, value, strength, fade in heads:
        key = key.astype(F32)
        key = key * lax.rsqrt(jnp.sum(key * key, axis=1, keepdims=True) + 1.0)
        weighted = (key * strength).astype(BF16)
        value = (value.astype(F32) * (strength * fade)).astype(BF16)
        key_t = key.astype(BF16).T
        half = weighted.shape[0] // 2
        keys_t.append(key_t)
        rights.append(jnp.concatenate([value, weighted], axis=1))
        grams.append(mul(jnp.concatenate([weighted[:half], weighted[half:]], axis=1), key_t))
    cuts = masks.shape[0]
    tick()
    ns = [g * masks[0] for g in grams]
    squares = [mul(x, x) for x in ns]
    tick()
    xs = [eye[...] - x for x in ns]
    pairs = [mul(under(q, x), q) for q, x in zip(squares, xs)]
    tick()
    xs = [x + p[half:] for x, p in zip(xs, pairs)]
    xs = [x + mul(x, p[:half]) for x, p in zip(xs, pairs)]
    for cut in range(1, cuts):
        tick()
        last = cut == cuts - 1
        if last:
            both = [mul(under(g * masks[cut], k), x) for g, k, x in zip(grams, keys_t, xs)]
            ns, xs = [b[:half] for b in both], [b[half:] for b in both]
        else:
            ns = [mul(g * masks[cut], x) for g, x in zip(grams, xs)]
        tick()
        pairs = [mul(under(q, x), q) for q, x in zip(ns, xs)]
        tick()
        xs = [x - p[half:] for x, p in zip(xs, pairs)]
        xs = [x + mul(x, p[:half]) for x, p in zip(xs, pairs)]
    if cuts == 1:
        tick()
        xs = [mul(k, x) for k, x in zip(keys_t, xs)]
    tick()
    first = [dot(x[:, :half], r[:half]) for x, r in zip(xs, rights)]
    second = [dot(x[:, half:], r[half:]) for x, r in zip(xs, rights)]
    tick()
    dim = keys_t[0].shape[0]
    out = [a + b - dot(b[:, dim:].astype(BF16), a.astype(BF16)) for a, b in zip(first, second)]
    tick()
    return out


def kernel(
    n, tp, groups, per, dim, together,
    prompt, key_w, value_w, beta_w, bias, decay, query, gain,
    state_out, read_out,
    feat, weights, total, projected, beta_buf, bias_buf, decay_buf, query_buf, gain_buf,
    mask_buf, eye_buf, strength_buf, spans, partner_spans, joined, recv,
    row_stage, row_recv, read_stage, read_recv,
    in_sem, beta_sem, feat_send, feat_recv, weight_sem, pair_send, pair_recv,
    map_send, map_recv, row_send, row_got, read_send, read_got,
):
    me = lax.axis_index("sp")
    core = lax.axis_index("tp")
    seg, part = prompt.shape[1], prompt.shape[2]
    wide = per * dim
    full = seg * n
    stride = n // groups
    half = groups // 2
    parity = lax.rem(me, 2)
    mine = me // stride
    steps = groups // together
    chunk = min(part, 1024)

    away = [half // 2] + [j for j in range(1, half) if j != half // 2] if half > 1 else []
    order = away + [0]
    sequence = [(0, order[0])]
    for j in range(half):
        if j + 1 < half:
            sequence.append((0, order[j + 1]))
        sequence.append((1, order[j]))
    plan = [range(step * together, (step + 1) * together) for step in range(steps)]

    def owner(g):
        return g * stride + (lax.rem(g, 2) if stride > 1 else 0)

    is_owner = me == owner(mine)

    def when_owner(work):
        if stride == 1:
            work()
        else:
            pl.when(is_owner)(work)

    def pair_at(j):
        return lax.rem(mine // 2 + j, half)

    def group_at(index):
        keep, j = sequence[index]
        return 2 * pair_at(j) + (parity if keep else 1 - parity)

    def features_of(d):
        return pl.ds(pl.multiple_of(lax.rem(core + d, tp) * part, part), part)

    def fetch(index, d):
        columns = pl.ds(pl.multiple_of(group_at(index) * wide, wide), wide)
        return [
            pltpu.make_async_copy(
                w.at[features_of(d), columns], weights.at[index, j, d], weight_sem.at[index, j, d]
            )
            for j, w in enumerate((key_w, value_w))
        ]

    def fetch_step(step):
        for d in range(tp):
            for index in plan[step]:
                for copy in fetch(index, d):
                    copy.start()

    own_prompt = pltpu.make_async_copy(prompt.at[0], feat.at[0], in_sem.at[0])
    small = [
        pltpu.make_async_copy(src, dst, in_sem.at[1 + k])
        for k, (src, dst) in enumerate(
            ((bias, bias_buf), (decay, decay_buf), (query, query_buf), (gain, gain_buf))
        )
    ] + [
        pltpu.make_async_copy(beta_w.at[:, features_of(d)], beta_buf.at[d], beta_sem.at[d]) for d in range(tp)
    ]
    own_prompt.start()
    fetch_step(0)
    for copy in small:
        copy.start()
    if steps > 1:
        fetch_step(1)

    barrier = pltpu.get_barrier_semaphore()
    for d in range(1, tp):
        pl.semaphore_signal(barrier, inc=1, device_id={"tp": lax.rem(core + d, tp)}, device_id_type=MESH)
    for d in range(1, n):
        pl.semaphore_signal(barrier, inc=1, device_id={"sp": lax.rem(me + d, n)}, device_id_type=MESH)
    masks, eye = cut_masks(seg // 2)
    for k, mask in enumerate(masks):
        mask_buf[k] = mask
    eye_buf[...] = eye
    own_prompt.wait()
    pl.semaphore_wait(barrier, n - 1 + tp - 1)

    def feature_copy(d):
        return pltpu.make_async_remote_copy(
            src_ref=feat.at[0], dst_ref=feat.at[tp - d],
            send_sem=feat_send.at[d - 1], recv_sem=feat_recv.at[tp - d],
            device_id={"tp": lax.rem(core + d, tp)}, device_id_type=MESH,
        )

    for d in range(1, tp):
        feature_copy(d).start()

    for index in plan[0]:
        for j, copy in enumerate(fetch(index, 0)):
            copy.wait()
            total[index, j] = dot(feat[0], weights[index, j, 0])
    for copy in small:
        copy.wait()
    before = dot(feat[0], beta_buf[0], ((1,), (1,)))
    for d in range(1, tp):
        feature_copy(tp - d).wait_recv()
        before += dot(feat[d], beta_buf[d], ((1,), (1,)))
    strength_buf[...] = jax.nn.sigmoid(before + bias_buf[...])
    for index in plan[0]:
        for d in range(1, tp):
            for copy in fetch(index, d):
                copy.wait()
    for index in plan[0]:
        for j in range(2):
            acc = total[index, j]
            for d in range(1, tp):
                acc += dot(feat[d], weights[index, j, d])
            projected[index, j] = acc.astype(BF16)

    def pair_copy(index, j):
        return pltpu.make_async_remote_copy(
            src_ref=spans.at[index], dst_ref=partner_spans.at[j],
            send_sem=pair_send.at[j], recv_sem=pair_recv.at[j],
            device_id={"sp": me + 1 - 2 * parity}, device_id_type=MESH,
        )

    def map_copy(j, slot):
        return pltpu.make_async_remote_copy(
            src_ref=joined.at[j], dst_ref=recv.at[slot],
            send_sem=map_send.at[j], recv_sem=map_recv.at[slot],
            device_id={"sp": owner(2 * pair_at(j) + parity)}, device_id_type=MESH,
        )

    def is_away(j):
        return owner(2 * pair_at(j) + parity) != me

    def pass_on(step):
        for index in plan[step]:
            keep, j = sequence[index]
            if not keep:
                pair_copy(index, j).start()
        for index in plan[step]:
            keep, j = sequence[index]
            if keep:
                pair_copy(index, j).wait_recv()
                for h in range(per):
                    ours, theirs = spans[index, h], partner_spans[j, h]
                    early = jnp.where(parity == 1, theirs, ours)
                    late = jnp.where(parity == 1, ours, theirs)
                    both = early.astype(F32) + late.astype(F32) - dot(late[:, dim:], early)
                    joined[j, h] = both.astype(BF16)
                if j or stride > 1:
                    @pl.when(is_away(j))
                    def _():
                        map_copy(j, me // 2).start()

    def projection(step):
        for index in plan[step]:
            for j in range(2):
                acc = None
                for d in range(tp):
                    for low in range(0, part, chunk):
                        piece = dot(
                            feat[d, :, low:low + chunk], weights[index, j, d, low:low + chunk, :]
                        )
                        acc = piece if acc is None else acc + piece
                        if d == tp - 1 and low + chunk == part:
                            projected[index, j] = acc.astype(BF16)
                        yield

    ticks = 2 + 3 * len(masks) + 1
    units = together * 2 * tp * (part // chunk)
    for step in range(steps):
        if step > 0:
            pass_on(step - 1)
        if step + 2 < steps:
            fetch_step(step + 2)
        filler = iter(())
        if step + 1 < steps:
            for index in plan[step + 1]:
                for d in range(tp):
                    for copy in fetch(index, d):
                        copy.wait()
            filler = projection(step + 1)
        done = [0, 0]

        def tick():
            done[0] += 1
            while done[1] * ticks < done[0] * units:
                done[1] += 1
                next(filler, None)

        strengths = strength_buf[...]
        rates = decay_buf[...]
        lane = lax.broadcasted_iota(jnp.int32, strengths.shape, 1)
        rest = full - 1 - me * seg - lax.broadcasted_iota(jnp.int32, (seg, 1), 0)
        rest = rest.astype(F32) * (1.0 / full)
        heads = []
        for index in plan[step]:
            keys, values = projected[index, 0], projected[index, 1]
            for h in range(per):
                head = group_at(index) * per + h
                strength = jnp.sum(jnp.where(lane == head, strengths, 0.0), axis=1, keepdims=True)
                rate = jnp.sum(jnp.where(lane[:1] == head, rates, 0.0), axis=1, keepdims=True)
                fade = jnp.exp(-rate * rest)
                cols = slice(h * dim, (h + 1) * dim)
                heads.append((keys[:, cols], values[:, cols], strength, fade))
        results = span(heads, mask_buf, eye_buf, tick)
        for _ in filler:
            pass
        for k, result in enumerate(results):
            spans[plan[step][k // per], k % per] = result.astype(BF16)
    pass_on(steps - 1)
    recv[me // 2] = joined[0]

    rows = dim // n

    def row_copy(q, slot):
        return pltpu.make_async_remote_copy(
            src_ref=row_stage.at[q], dst_ref=row_recv.at[slot],
            send_sem=row_send.at[q], recv_sem=row_got.at[slot],
            device_id={"sp": q}, device_id_type=MESH,
        )

    def read_copy(q, slot):
        return pltpu.make_async_remote_copy(
            src_ref=read_stage, dst_ref=read_recv.at[slot],
            send_sem=read_send.at[q], recv_sem=read_got.at[slot],
            device_id={"sp": q}, device_id_type=MESH,
        )

    def finish():
        def link(p, states):
            @pl.when(p != me // 2)
            def _():
                map_copy(0, p).wait_recv()

            new = []
            for h in range(per):
                write, drop = recv[p, h, :, :dim].astype(F32), recv[p, h, :, dim:]
                high = states[h].astype(BF16)
                low = (states[h] - high.astype(F32)).astype(BF16)
                new.append(states[h] + (write - dot(drop, high) - dot(drop, low)))
            return tuple(new)

        states = lax.fori_loop(0, n // 2, link, tuple(jnp.zeros((dim, dim), F32) for _ in range(per)))
        for h in range(per):
            cast = states[h].astype(BF16)
            for q in range(n):
                row_stage[q, h] = cast[q * rows:(q + 1) * rows]
        unit = query_buf[0].astype(F32)
        unit = unit * lax.rsqrt(jnp.sum(unit * unit, axis=1, keepdims=True) + 1.0)
        which = lax.broadcasted_iota(jnp.int32, unit.shape, 0)
        for h in range(per):
            row = jnp.sum(jnp.where(which == mine * per + h, unit, 0.0), axis=0, keepdims=True)
            raw = jnp.dot(
                jnp.broadcast_to(row, (8, dim)), states[h],
                precision=lax.Precision.HIGHEST, preferred_element_type=F32,
            )[0:1]
            raw = raw * lax.rsqrt(jnp.mean(raw * raw, axis=1, keepdims=True) + 0.05) * gain_buf[...]
            read_stage[h:h + 1] = raw
        for d in range(1, n):
            row_copy(lax.rem(me + d, n), mine).start()
        for d in range(1, n):
            read_copy(lax.rem(me + d, n), mine).start()
        row_recv[mine] = row_stage[me]
        read_recv[mine] = read_stage[...]

    when_owner(finish)

    for g in range(groups):
        @pl.when(me != owner(g))
        def _():
            row_copy(me, g).wait_recv()
            read_copy(me, g).wait_recv()

        for h in range(per):
            state_out[0, g * per + h] = row_recv[g, h]
        read_out[0, g * per:(g + 1) * per] = read_recv[g]

    for d in range(1, tp):
        feature_copy(d).wait_send()
    for j in range(half):
        pair_copy(0, j).wait_send()
        if j or stride > 1:
            @pl.when(is_away(j))
            def _():
                map_copy(j, 0).wait_send()

    def sent():
        for d in range(1, n):
            row_copy(lax.rem(me + d, n), mine).wait_send()
            read_copy(lax.rem(me + d, n), mine).wait_send()

    when_owner(sent)


def solution(mesh):
    n, tp = mesh.shape["sp"], mesh.shape["tp"]

    def shards(prompt, key_w, value_w, beta_w, bias, decay, query, gain):
        seg, part = prompt.shape[1:]
        depth = key_w.shape[0]
        heads = beta_w.shape[1]
        dim = key_w.shape[1] // heads
        per = max(1, heads // n)
        groups = heads // per
        wide = per * dim
        rows = dim // n
        block = seg // 2
        cuts = len(bounds(block))
        dma = pltpu.SemaphoreType.DMA
        vmem = pl.BlockSpec(memory_space=pltpu.VMEM)
        hbm = pl.BlockSpec(memory_space=pl.ANY)
        half = groups // 2
        together = min(2, groups)
        return pl.pallas_call(
            functools.partial(kernel, n, tp, groups, per, dim, together),
            out_shape=(
                jax.ShapeDtypeStruct((1, heads, rows, dim), BF16),
                jax.ShapeDtypeStruct((1, heads, dim), F32),
            ),
            in_specs=[hbm] * 8,
            out_specs=(vmem, vmem),
            scratch_shapes=[
                pltpu.VMEM((tp, seg, part), BF16),
                pltpu.VMEM((groups, 2, tp, part, wide), BF16),
                pltpu.VMEM((together, 2, seg, wide), F32),
                pltpu.VMEM((groups, 2, seg, wide), BF16),
                pltpu.VMEM((tp, heads, part), BF16),
                pltpu.VMEM((1, heads), F32),
                pltpu.VMEM((1, heads), F32),
                pltpu.VMEM((1, heads, dim), BF16),
                pltpu.VMEM((1, dim), F32),
                pltpu.VMEM((cuts, block, seg), BF16),
                pltpu.VMEM((block, seg), BF16),
                pltpu.VMEM((seg, heads), F32),
                pltpu.VMEM((groups, per, dim, 2 * dim), BF16),
                pltpu.VMEM((half, per, dim, 2 * dim), BF16),
                pltpu.VMEM((half, per, dim, 2 * dim), BF16),
                pltpu.VMEM((n // 2, per, dim, 2 * dim), BF16),
                pltpu.VMEM((n, per, rows, dim), BF16),
                pltpu.VMEM((groups, per, rows, dim), BF16),
                pltpu.VMEM((per, dim), F32),
                pltpu.VMEM((groups, per, dim), F32),
                dma((5,)),
                dma((tp,)),
                dma((tp - 1,)),
                dma((tp,)),
                dma((groups, 2, tp)),
                dma((half,)),
                dma((half,)),
                dma((half,)),
                dma((n // 2,)),
                dma((n,)),
                dma((groups,)),
                dma((n,)),
                dma((groups,)),
            ],
            compiler_params=pltpu.CompilerParams(
                collective_id=0, has_side_effects=True, vmem_limit_bytes=60 * 2**20
            ),
        )(
            prompt, key_w, value_w, beta_w.T, bias.reshape(1, heads), decay.reshape(1, heads),
            query, gain.reshape(1, dim),
        )

    return jax.shard_map(
        shards,
        mesh=mesh,
        in_specs=(
            P("gr", "sp", "tp"),
            P(None, "tp"),
            P(None, "tp"),
            P(None, "tp"),
            P("tp"),
            P("tp"),
            P("gr", "tp", None),
            P(),
        ),
        out_specs=(P("gr", "tp", "sp", None), P("gr", "tp", None)),
        check_vma=False,
    )
```

time: 52.8 us -> 45.1 us (0.85)
  Pallas kernels: 49.1 us -> 41.5 us
    pallas_call x1, Pallas kernels: 49.1 us -> 41.5 us  [shards(): pl.pallas_call(functools.partial(kernel, n, tp, groups, per, dim, togethe...]
where the time goes in v1:
time: 45.1 us; the launch traced here: 44.9 us
  Pallas kernels  41.5 us (92%)
  local copies, waits for them, and re-layouts  2.77 us (6%)
  between operations  0.64 us (1%)
    pallas_call x1, Pallas kernels, shards(): pl.pallas_call(functools.partial(kernel, n, tp, groups, per, dim, togethe...  41.5 us
    unnamed x2, local copies, waits for them, and re-layouts  2.77 us

profile of v1, /device:TPU:0, one launch (start us, length us, event | category | flops | bytes accessed | tf_op | source)
XLA Modules:
  0.0 44.9 jit_solution(3134009427610583905)
XLA Ops:
  0.6 41.5 %shard_map.95 = (bf16[1,16,16,128]{3,2,1,0:T(8,128)(2,1)}, f32[1,16,128]{2,1,0:T(8,128)}) custom-call(bf16[1,256,2048]{2,1,0:T(8,128)(2,1)} %prompt.1, bf16[4096,2048]{1,0:T(8,128)(2,1)} %key_w.1, bf16[4096,2048]{1,0:T(8,128)(2,1)} %value_w.1, bf16[16,4096]{1,0:T(8,128)(2,1)} %bitcast.4, f32[1,16]{1,0:T(1,128)} %bitcast.5, f32[1,16]{1,0:T(1,128)} %bitcast.6, ...), custom_call_target="tpu_custom_call" | custom-call | tf_op jit(solution)/shard_map/pallas_call | solution.py:426
  42.1 1.5 %copy.12 = bf16[1,16,16,128]{3,2,1,0:T(8,128)(2,1)} copy(bf16[1,16,16,128]{3,2,1,0:T(8,128)(2,1)} %get-tuple-element.4) | data formatting | bytes 131072
  43.6 1.3 %copy.13 = f32[1,16,128]{2,1,0:T(8,128)} copy(f32[1,16,128]{2,1,0:T(8,128)} %get-tuple-element.5) | data formatting | bytes 16384

commit v2 on v1

--- a/solution.py
+++ b/solution.py
@@ -100,7 +100,7 @@
 
 
 def kernel(
-    n, tp, groups, per, dim, together,
+    n, tp, groups, per, dim,
     prompt, key_w, value_w, beta_w, bias, decay, query, gain,
     state_out, read_out,
     feat, weights, total, projected, beta_buf, bias_buf, decay_buf, query_buf, gain_buf,
@@ -118,17 +118,17 @@
     half = groups // 2
     parity = lax.rem(me, 2)
     mine = me // stride
-    steps = groups // together
     chunk = min(part, 1024)
 
-    away = [half // 2] + [j for j in range(1, half) if j != half // 2] if half > 1 else []
-    order = away + [0]
+    order = list(range(half // 2, half)) + list(range(half // 2 - 1, -1, -1))
     sequence = [(0, order[0])]
     for j in range(half):
         if j + 1 < half:
             sequence.append((0, order[j + 1]))
         sequence.append((1, order[j]))
-    plan = [range(step * together, (step + 1) * together) for step in range(steps)]
+    plan = [range(1)] + [range(k, k + 2) for k in range(1, groups - 1, 2)] + [range(groups - 1, groups)]
+    steps = len(plan)
+    early = 1 + len(plan[1])
 
     def owner(g):
         return g * stride + (lax.rem(g, 2) if stride > 1 else 0)
@@ -142,7 +142,14 @@
             pl.when(is_owner)(work)
 
     def pair_at(j):
-        return lax.rem(mine // 2 + j, half)
+        pair = mine // 2
+        if half & (half - 1):
+            return lax.rem(pair + j, half)
+        place = pair
+        for bit in range(half.bit_length()):
+            if j >> bit & 1:
+                place += (1 - 2 * lax.rem(pair // 2**bit, 2)) * 2**bit
+        return place
 
     def group_at(index):
         keep, j = sequence[index]
@@ -160,8 +167,8 @@
             for j, w in enumerate((key_w, value_w))
         ]
 
-    def fetch_step(step):
-        for d in range(tp):
+    def fetch_step(step, ds=None):
+        for d in ds or range(tp):
             for index in plan[step]:
                 for copy in fetch(index, d):
                     copy.start()
@@ -176,11 +183,10 @@
         pltpu.make_async_copy(beta_w.at[:, features_of(d)], beta_buf.at[d], beta_sem.at[d]) for d in range(tp)
     ]
     own_prompt.start()
-    fetch_step(0)
+    fetch_step(0, range(1))
     for copy in small:
         copy.start()
-    if steps > 1:
-        fetch_step(1)
+    fetch_step(1, range(1))
 
     barrier = pltpu.get_barrier_semaphore()
     for d in range(1, tp):
@@ -203,22 +209,33 @@
 
     for d in range(1, tp):
         feature_copy(d).start()
-
-    for index in plan[0]:
-        for j, copy in enumerate(fetch(index, 0)):
-            copy.wait()
-            total[index, j] = dot(feat[0], weights[index, j, 0])
+    fetch_step(0, range(1, tp))
+    fetch_step(1, range(1, tp))
+
+    def begin(step):
+        for index in plan[step]:
+            for copy in fetch(index, 0):
+                copy.wait()
+        for index in plan[step]:
+            for j in range(2):
+                total[index, j] = dot(feat[0], weights[index, j, 0])
+
+    begin(0)
+    if steps > 2:
+        fetch_step(2)
     for copy in small:
         copy.wait()
+    begin(1)
     before = dot(feat[0], beta_buf[0], ((1,), (1,)))
-    for d in range(1, tp):
-        feature_copy(tp - d).wait_recv()
-        before += dot(feat[d], beta_buf[d], ((1,), (1,)))
-    strength_buf[...] = jax.nn.sigmoid(before + bias_buf[...])
     for index in plan[0]:
         for d in range(1, tp):
             for copy in fetch(index, d):
                 copy.wait()
+    for d in range(1, tp):
+        feature_copy(tp - d).wait_recv()
+    for d in range(1, tp):
+        before += dot(feat[d], beta_buf[d], ((1,), (1,)))
+    strength_buf[...] = jax.nn.sigmoid(before + bias_buf[...])
     for index in plan[0]:
         for j in range(2):
             acc = total[index, j]
@@ -266,8 +283,8 @@
     def projection(step):
         for index in plan[step]:
             for j in range(2):
-                acc = None
-                for d in range(tp):
+                acc = total[index, j] if index < early else None
+                for d in range(1 if index < early else 0, tp):
                     for low in range(0, part, chunk):
                         piece = dot(
                             feat[d, :, low:low + chunk], weights[index, j, d, low:low + chunk, :]
@@ -278,16 +295,17 @@
                         yield
 
     ticks = 2 + 3 * len(masks) + 1
-    units = together * 2 * tp * (part // chunk)
     for step in range(steps):
         if step > 0:
             pass_on(step - 1)
-        if step + 2 < steps:
+        if 2 < step + 2 < steps:
             fetch_step(step + 2)
-        filler = iter(())
+        filler, units = iter(()), 0
         if step + 1 < steps:
+            skip = 1 if step == 0 else 0
+            units = len(plan[step + 1]) * 2 * (tp - skip) * (part // chunk)
             for index in plan[step + 1]:
-                for d in range(tp):
+                for d in range(skip, tp):
                     for copy in fetch(index, d):
                         copy.wait()
             filler = projection(step + 1)
@@ -318,7 +336,7 @@
         for _ in filler:
             pass
         for k, result in enumerate(results):
-            spans[plan[step][k // per], k % per] = result.astype(BF16)
+            spans[plan[step][0] + k // per, k % per] = result.astype(BF16)
     pass_on(steps - 1)
     recv[me // 2] = joined[0]
 
@@ -339,37 +357,38 @@
         )
 
     def finish():
-        def link(p, states):
+        unit = query_buf[0].astype(F32)
+        unit = unit * lax.rsqrt(jnp.sum(unit * unit, axis=1, keepdims=True) + 1.0)
+        which = lax.broadcasted_iota(jnp.int32, unit.shape, 0)
+        asks = []
+        for h in range(per):
+            row = jnp.sum(jnp.where(which == mine * per + h, unit, 0.0), axis=0, keepdims=True)
+            asks.append(jnp.broadcast_to(row, (dim, dim)).T)
+
+        def arrive(p):
             @pl.when(p != me // 2)
             def _():
                 map_copy(0, p).wait_recv()
 
-            new = []
+        arrive(0)
+        states = [recv[0, h, :, :dim].astype(F32) for h in range(per)]
+        for p in range(1, n // 2):
+            arrive(p)
             for h in range(per):
                 write, drop = recv[p, h, :, :dim].astype(F32), recv[p, h, :, dim:]
                 high = states[h].astype(BF16)
                 low = (states[h] - high.astype(F32)).astype(BF16)
-                new.append(states[h] + (write - dot(drop, high) - dot(drop, low)))
-            return tuple(new)
-
-        states = lax.fori_loop(0, n // 2, link, tuple(jnp.zeros((dim, dim), F32) for _ in range(per)))
+                states[h] = states[h] + (write - dot(drop, high) - dot(drop, low))
         for h in range(per):
             cast = states[h].astype(BF16)
             for q in range(n):
                 row_stage[q, h] = cast[q * rows:(q + 1) * rows]
-        unit = query_buf[0].astype(F32)
-        unit = unit * lax.rsqrt(jnp.sum(unit * unit, axis=1, keepdims=True) + 1.0)
-        which = lax.broadcasted_iota(jnp.int32, unit.shape, 0)
+        for d in range(n - 1, 0, -1):
+            row_copy(lax.rem(me + d, n), mine).start()
         for h in range(per):
-            row = jnp.sum(jnp.where(which == mine * per + h, unit, 0.0), axis=0, keepdims=True)
-            raw = jnp.dot(
-                jnp.broadcast_to(row, (8, dim)), states[h],
-                precision=lax.Precision.HIGHEST, preferred_element_type=F32,
-            )[0:1]
+            raw = jnp.sum(asks[h] * states[h], axis=0, keepdims=True)
             raw = raw * lax.rsqrt(jnp.mean(raw * raw, axis=1, keepdims=True) + 0.05) * gain_buf[...]
             read_stage[h:h + 1] = raw
-        for d in range(1, n):
-            row_copy(lax.rem(me + d, n), mine).start()
         for d in range(1, n):
             read_copy(lax.rem(me + d, n), mine).start()
         row_recv[mine] = row_stage[me]
@@ -422,19 +441,18 @@
         vmem = pl.BlockSpec(memory_space=pltpu.VMEM)
         hbm = pl.BlockSpec(memory_space=pl.ANY)
         half = groups // 2
-        together = min(2, groups)
         return pl.pallas_call(
-            functools.partial(kernel, n, tp, groups, per, dim, together),
+            functools.partial(kernel, n, tp, groups, per, dim),
             out_shape=(
-                jax.ShapeDtypeStruct((1, heads, rows, dim), BF16),
-                jax.ShapeDtypeStruct((1, heads, dim), F32),
+                pltpu.VMEM((1, heads, rows, dim), BF16),
+                pltpu.VMEM((1, heads, dim), F32),
             ),
             in_specs=[hbm] * 8,
             out_specs=(vmem, vmem),
             scratch_shapes=[
                 pltpu.VMEM((tp, seg, part), BF16),
                 pltpu.VMEM((groups, 2, tp, part, wide), BF16),
-                pltpu.VMEM((together, 2, seg, wide), F32),
+                pltpu.VMEM((3, 2, seg, wide), F32),
                 pltpu.VMEM((groups, 2, seg, wide), BF16),
                 pltpu.VMEM((tp, heads, part), BF16),
                 pltpu.VMEM((1, heads), F32),

time: 45.1 us -> 38.7 us (0.86)
  Pallas kernels: 41.5 us -> 36.7 us
  local copies, waits for them, and re-layouts: 2.77 us -> 1.23 us
    pallas_call x1, Pallas kernels: 41.5 us -> 36.7 us  [shards(): pl.pallas_call(functools.partial(kernel, n, tp, groups, per, dim), out_sh...]
    unnamed x2, local copies, waits for them, and re-layouts: 2.77 us -> 1.23 us
where the time goes in v2:
time: 38.7 us; the launch traced here: 38.6 us
  Pallas kernels  36.7 us (95%)
  local copies, waits for them, and re-layouts  1.23 us (3%)
  between operations  0.64 us (2%)
    pallas_call x1, Pallas kernels, shards(): pl.pallas_call(functools.partial(kernel, n, tp, groups, per, dim), out_sh...  36.7 us
    unnamed x2, local copies, waits for them, and re-layouts  1.23 us

profile of v2, /device:TPU:0, one launch (start us, length us, event | category | flops | bytes accessed | tf_op | source)
XLA Modules:
  0.0 38.6 jit_solution(9161505285632834513)
XLA Ops:
  0.6 36.7 %shard_map.95 = (bf16[1,16,16,128]{3,2,1,0:T(8,128)(2,1)S(1)}, f32[1,16,128]{2,1,0:T(8,128)S(1)}) custom-call(bf16[1,256,2048]{2,1,0:T(8,128)(2,1)} %prompt.1, bf16[4096,2048]{1,0:T(8,128)(2,1)} %key_w.1, bf16[4096,2048]{1,0:T(8,128)(2,1)} %value_w.1, bf16[16,4096]{1,0:T(8,128)(2,1)} %bitcast.4, f32[1,16]{1,0:T(1,128)} %bitcast.5, f32[1,16]{1,0:T(1,128)} %bitcast.6, ...), custom_call_target="tpu_custom_call" | custom-call | tf_op jit(solution)/shard_map/pallas_call | solution.py:444
  37.3 0.6 %copy.12 = bf16[1,16,16,128]{3,2,1,0:T(8,128)(2,1)} copy(bf16[1,16,16,128]{3,2,1,0:T(8,128)(2,1)S(1)} %get-tuple-element.2) | data formatting | bytes 131072
  38.0 0.6 %copy.13 = f32[1,16,128]{2,1,0:T(8,128)} copy(f32[1,16,128]{2,1,0:T(8,128)S(1)} %get-tuple-element.3) | data formatting | bytes 16384

commit v3 on v2

--- a/solution.py
+++ b/solution.py
@@ -105,7 +105,7 @@
     state_out, read_out,
     feat, weights, total, projected, beta_buf, bias_buf, decay_buf, query_buf, gain_buf,
     mask_buf, eye_buf, strength_buf, spans, partner_spans, joined, recv,
-    row_stage, row_recv, read_stage, read_recv,
+    ask_buf, row_stage, read_stage, read_recv,
     in_sem, beta_sem, feat_send, feat_recv, weight_sem, pair_send, pair_recv,
     map_send, map_recv, row_send, row_got, read_send, read_got,
 ):
@@ -158,20 +158,19 @@
     def features_of(d):
         return pl.ds(pl.multiple_of(lax.rem(core + d, tp) * part, part), part)
 
-    def fetch(index, d):
-        columns = pl.ds(pl.multiple_of(group_at(index) * wide, wide), wide)
-        return [
-            pltpu.make_async_copy(
-                w.at[features_of(d), columns], weights.at[index, j, d], weight_sem.at[index, j, d]
-            )
-            for j, w in enumerate((key_w, value_w))
-        ]
-
-    def fetch_step(step, ds=None):
-        for d in ds or range(tp):
+    def fetch_step(step, low, high):
+        for d in range(low, high):
             for index in plan[step]:
-                for copy in fetch(index, d):
-                    copy.start()
+                columns = pl.ds(pl.multiple_of(group_at(index) * wide, wide), wide)
+                for j, w in enumerate((key_w, value_w)):
+                    pltpu.make_async_copy(
+                        w.at[features_of(d), columns], weights.at[index, d, j],
+                        weight_sem.at[step, min(low, 1)],
+                    ).start()
+
+    def fetched(step, low, high):
+        landed = weights.at[plan[step][0]:plan[step][-1] + 1, low:high]
+        pltpu.make_async_copy(landed, landed, weight_sem.at[step, min(low, 1)]).wait()
 
     own_prompt = pltpu.make_async_copy(prompt.at[0], feat.at[0], in_sem.at[0])
     small = [
@@ -183,10 +182,10 @@
         pltpu.make_async_copy(beta_w.at[:, features_of(d)], beta_buf.at[d], beta_sem.at[d]) for d in range(tp)
     ]
     own_prompt.start()
-    fetch_step(0, range(1))
     for copy in small:
         copy.start()
-    fetch_step(1, range(1))
+    fetch_step(0, 0, 1)
+    fetch_step(1, 0, 1)
 
     barrier = pltpu.get_barrier_semaphore()
     for d in range(1, tp):
@@ -209,28 +208,23 @@
 
     for d in range(1, tp):
         feature_copy(d).start()
-    fetch_step(0, range(1, tp))
-    fetch_step(1, range(1, tp))
+    fetch_step(0, 1, tp)
+    fetch_step(1, 1, tp)
 
     def begin(step):
-        for index in plan[step]:
-            for copy in fetch(index, 0):
-                copy.wait()
+        fetched(step, 0, 1)
         for index in plan[step]:
             for j in range(2):
-                total[index, j] = dot(feat[0], weights[index, j, 0])
-
-    begin(0)
-    if steps > 2:
-        fetch_step(2)
+                total[index, j] = dot(feat[0], weights[index, 0, j])
+
     for copy in small:
         copy.wait()
+    before = dot(feat[0], beta_buf[0], ((1,), (1,)))
+    begin(0)
     begin(1)
-    before = dot(feat[0], beta_buf[0], ((1,), (1,)))
-    for index in plan[0]:
-        for d in range(1, tp):
-            for copy in fetch(index, d):
-                copy.wait()
+    if steps > 2:
+        fetch_step(2, 0, tp)
+    fetched(0, 1, tp)
     for d in range(1, tp):
         feature_copy(tp - d).wait_recv()
     for d in range(1, tp):
@@ -240,20 +234,20 @@
         for j in range(2):
             acc = total[index, j]
             for d in range(1, tp):
-                acc += dot(feat[d], weights[index, j, d])
+                acc += dot(feat[d], weights[index, d, j])
             projected[index, j] = acc.astype(BF16)
 
     def pair_copy(index, j):
         return pltpu.make_async_remote_copy(
             src_ref=spans.at[index], dst_ref=partner_spans.at[j],
-            send_sem=pair_send.at[j], recv_sem=pair_recv.at[j],
+            send_sem=pair_send, recv_sem=pair_recv.at[j],
             device_id={"sp": me + 1 - 2 * parity}, device_id_type=MESH,
         )
 
     def map_copy(j, slot):
         return pltpu.make_async_remote_copy(
             src_ref=joined.at[j], dst_ref=recv.at[slot],
-            send_sem=map_send.at[j], recv_sem=map_recv.at[slot],
+            send_sem=map_send, recv_sem=map_recv.at[slot],
             device_id={"sp": owner(2 * pair_at(j) + parity)}, device_id_type=MESH,
         )
 
@@ -287,7 +281,7 @@
                 for d in range(1 if index < early else 0, tp):
                     for low in range(0, part, chunk):
                         piece = dot(
-                            feat[d, :, low:low + chunk], weights[index, j, d, low:low + chunk, :]
+                            feat[d, :, low:low + chunk], weights[index, d, j, low:low + chunk, :]
                         )
                         acc = piece if acc is None else acc + piece
                         if d == tp - 1 and low + chunk == part:
@@ -299,15 +293,12 @@
         if step > 0:
             pass_on(step - 1)
         if 2 < step + 2 < steps:
-            fetch_step(step + 2)
+            fetch_step(step + 2, 0, tp)
         filler, units = iter(()), 0
         if step + 1 < steps:
             skip = 1 if step == 0 else 0
             units = len(plan[step + 1]) * 2 * (tp - skip) * (part // chunk)
-            for index in plan[step + 1]:
-                for d in range(skip, tp):
-                    for copy in fetch(index, d):
-                        copy.wait()
+            fetched(step + 1, skip, tp)
             filler = projection(step + 1)
         done = [0, 0]
 
@@ -337,34 +328,32 @@
             pass
         for k, result in enumerate(results):
             spans[plan[step][0] + k // per, k % per] = result.astype(BF16)
+    rows = dim // n
+
+    def row_copy(q):
+        return pltpu.make_async_remote_copy(
+            src_ref=row_stage.at[q], dst_ref=state_out.at[0, pl.ds(mine * per, per)],
+            send_sem=row_send, recv_sem=row_got,
+            device_id={"sp": q}, device_id_type=MESH,
+        )
+
+    def read_copy(q):
+        return pltpu.make_async_remote_copy(
+            src_ref=read_stage.at[q], dst_ref=read_recv.at[mine],
+            send_sem=read_send, recv_sem=read_got,
+            device_id={"sp": q}, device_id_type=MESH,
+        )
+
+    unit = query_buf[0].astype(F32)
+    unit = unit * lax.rsqrt(jnp.sum(unit * unit, axis=1, keepdims=True) + 1.0)
+    which = lax.broadcasted_iota(jnp.int32, unit.shape, 0)
+    for h in range(per):
+        row = jnp.sum(jnp.where(which == mine * per + h, unit, 0.0), axis=0, keepdims=True)
+        ask_buf[h] = jnp.broadcast_to(row, (dim, dim)).T
     pass_on(steps - 1)
     recv[me // 2] = joined[0]
 
-    rows = dim // n
-
-    def row_copy(q, slot):
-        return pltpu.make_async_remote_copy(
-            src_ref=row_stage.at[q], dst_ref=row_recv.at[slot],
-            send_sem=row_send.at[q], recv_sem=row_got.at[slot],
-            device_id={"sp": q}, device_id_type=MESH,
-        )
-
-    def read_copy(q, slot):
-        return pltpu.make_async_remote_copy(
-            src_ref=read_stage, dst_ref=read_recv.at[slot],
-            send_sem=read_send.at[q], recv_sem=read_got.at[slot],
-            device_id={"sp": q}, device_id_type=MESH,
-        )
-
     def finish():
-        unit = query_buf[0].astype(F32)
-        unit = unit * lax.rsqrt(jnp.sum(unit * unit, axis=1, keepdims=True) + 1.0)
-        which = lax.broadcasted_iota(jnp.int32, unit.shape, 0)
-        asks = []
-        for h in range(per):
-            row = jnp.sum(jnp.where(which == mine * per + h, unit, 0.0), axis=0, keepdims=True)
-            asks.append(jnp.broadcast_to(row, (dim, dim)).T)
-
         def arrive(p):
             @pl.when(p != me // 2)
             def _():
@@ -384,43 +373,60 @@
             for q in range(n):
                 row_stage[q, h] = cast[q * rows:(q + 1) * rows]
         for d in range(n - 1, 0, -1):
-            row_copy(lax.rem(me + d, n), mine).start()
+            row_copy(lax.rem(me + d, n)).start()
         for h in range(per):
-            raw = jnp.sum(asks[h] * states[h], axis=0, keepdims=True)
+            raw = jnp.sum(ask_buf[h] * states[h], axis=0, keepdims=True)
             raw = raw * lax.rsqrt(jnp.mean(raw * raw, axis=1, keepdims=True) + 0.05) * gain_buf[...]
-            read_stage[h:h + 1] = raw
+            for q in range(n):
+                read_stage[q, h:h + 1] = raw
         for d in range(1, n):
-            read_copy(lax.rem(me + d, n), mine).start()
-        row_recv[mine] = row_stage[me]
-        read_recv[mine] = read_stage[...]
+            read_copy(lax.rem(me + d, n)).start()
+        state_out[0, pl.ds(mine * per, per)] = row_stage[me]
+        read_recv[mine] = read_stage[0]
 
     when_owner(finish)
 
+    def wait_all(count):
+        rows_in, reads_in = state_out.at[0, :count * per], read_recv.at[:count]
+        pltpu.make_async_copy(rows_in, rows_in, row_got).wait()
+        pltpu.make_async_copy(reads_in, reads_in, read_got).wait()
+
+    def wait_sent():
+        for done, sem in ((row_stage.at[1:], row_send), (read_stage.at[1:], read_send)):
+            pltpu.make_async_copy(done, done, sem).wait()
+
+    def wait_maps(low):
+        if low < half:
+            done = joined.at[low:]
+            pltpu.make_async_copy(done, done, map_send).wait()
+
+    if stride == 1:
+        wait_all(groups - 1)
+    else:
+        pl.when(is_owner)(lambda: wait_all(groups - 1))
+        pl.when(jnp.logical_not(is_owner))(lambda: wait_all(groups))
     for g in range(groups):
-        @pl.when(me != owner(g))
-        def _():
-            row_copy(me, g).wait_recv()
-            read_copy(me, g).wait_recv()
-
-        for h in range(per):
-            state_out[0, g * per + h] = row_recv[g, h]
         read_out[0, g * per:(g + 1) * per] = read_recv[g]
-
     for d in range(1, tp):
         feature_copy(d).wait_send()
-    for j in range(half):
-        pair_copy(0, j).wait_send()
-        if j or stride > 1:
-            @pl.when(is_away(j))
-            def _():
-                map_copy(j, 0).wait_send()
-
-    def sent():
-        for d in range(1, n):
-            row_copy(lax.rem(me + d, n), mine).wait_send()
-            read_copy(lax.rem(me + d, n), mine).wait_send()
-
-    when_owner(sent)
+    pltpu.make_async_copy(partner_spans, partner_spans, pair_send).wait()
+    if stride == 1:
+        wait_maps(1)
+    else:
+        pl.when(is_owner)(lambda: wait_maps(1))
+        pl.when(jnp.logical_not(is_owner))(lambda: wait_maps(0))
+    when_owner(wait_sent)
+
+
+def deliver(state, read, state_out, read_out, sem):
+    copies = [
+        pltpu.make_async_copy(src, dst, sem.at[k])
+        for k, (src, dst) in enumerate(((state, state_out), (read, read_out)))
+    ]
+    for copy in copies:
+        copy.start()
+    for copy in copies:
+        copy.wait()
 
 
 def solution(mesh):
@@ -441,7 +447,7 @@
         vmem = pl.BlockSpec(memory_space=pltpu.VMEM)
         hbm = pl.BlockSpec(memory_space=pl.ANY)
         half = groups // 2
-        return pl.pallas_call(
+        found = pl.pallas_call(
             functools.partial(kernel, n, tp, groups, per, dim),
             out_shape=(
                 pltpu.VMEM((1, heads, rows, dim), BF16),
@@ -451,7 +457,7 @@
             out_specs=(vmem, vmem),
             scratch_shapes=[
                 pltpu.VMEM((tp, seg, part), BF16),
-                pltpu.VMEM((groups, 2, tp, part, wide), BF16),
+                pltpu.VMEM((groups, tp, 2, part, wide), BF16),
                 pltpu.VMEM((3, 2, seg, wide), F32),
                 pltpu.VMEM((groups, 2, seg, wide), BF16),
                 pltpu.VMEM((tp, heads, part), BF16),
@@ -466,23 +472,23 @@
                 pltpu.VMEM((half, per, dim, 2 * dim), BF16),
                 pltpu.VMEM((half, per, dim, 2 * dim), BF16),
                 pltpu.VMEM((n // 2, per, dim, 2 * dim), BF16),
+                pltpu.VMEM((per, dim, dim), F32),
                 pltpu.VMEM((n, per, rows, dim), BF16),
-                pltpu.VMEM((groups, per, rows, dim), BF16),
-                pltpu.VMEM((per, dim), F32),
+                pltpu.VMEM((n, per, dim), F32),
                 pltpu.VMEM((groups, per, dim), F32),
                 dma((5,)),
                 dma((tp,)),
                 dma((tp - 1,)),
                 dma((tp,)),
-                dma((groups, 2, tp)),
+                dma((groups // 2 + 1, 2)),
+                pltpu.SemaphoreType.DMA,
                 dma((half,)),
-                dma((half,)),
-                dma((half,)),
+                pltpu.SemaphoreType.DMA,
                 dma((n // 2,)),
-                dma((n,)),
-                dma((groups,)),
-                dma((n,)),
-                dma((groups,)),
+                pltpu.SemaphoreType.DMA,
+                pltpu.SemaphoreType.DMA,
+                pltpu.SemaphoreType.DMA,
+                pltpu.SemaphoreType.DMA,
             ],
             compiler_params=pltpu.CompilerParams(
                 collective_id=0, has_side_effects=True, vmem_limit_bytes=60 * 2**20
@@ -491,6 +497,13 @@
             prompt, key_w, value_w, beta_w.T, bias.reshape(1, heads), decay.reshape(1, heads),
             query, gain.reshape(1, dim),
         )
+        return pl.pallas_call(
+            deliver,
+            out_shape=tuple(jax.ShapeDtypeStruct(x.shape, x.dtype) for x in found),
+            in_specs=[vmem] * 2,
+            out_specs=(hbm, hbm),
+            scratch_shapes=[dma((2,))],
+        )(*(pltpu.with_memory_space_constraint(x, pltpu.VMEM) for x in found))
 
     return jax.shard_map(
         shards,

time: 38.7 us -> 37.8 us (0.977)
  local copies, waits for them, and re-layouts: 1.23 us -> 0 us
    unnamed x2 -> x0, local copies, waits for them, and re-layouts: 1.23 us -> none
    pallas_call x0 -> x1, Pallas kernels: none -> 0.65 us  [shards(): pl.pallas_call(deliver, out_shape=tuple((jax.ShapeDtypeStruct(x.shape, x....]
    pallas_call x1, Pallas kernels: 36.7 us -> 36.1 us  [shards(): pl.pallas_call(functools.partial(kernel, n, tp, groups, per, dim), out_sh...]
where the time goes in v3:
time: 37.8 us; the launch traced here: 37.6 us
  Pallas kernels  36.8 us (97%)
  between operations  0.8 us (2%)
    pallas_call x1, Pallas kernels, shards(): pl.pallas_call(functools.partial(kernel, n, tp, groups, per, dim), out_sh...  36.1 us

profile of v3, /device:TPU:0, one launch (start us, length us, event | category | flops | bytes accessed | tf_op | source)
XLA Modules:
  0.0 37.6 jit_solution(11531620491865503323)
XLA Ops:
  0.6 36.1 %shard_map.95 = (bf16[1,16,16,128]{3,2,1,0:T(8,128)(2,1)S(1)}, f32[1,16,128]{2,1,0:T(8,128)S(1)}) custom-call(bf16[1,256,2048]{2,1,0:T(8,128)(2,1)} %prompt.1, bf16[4096,2048]{1,0:T(8,128)(2,1)} %key_w.1, bf16[4096,2048]{1,0:T(8,128)(2,1)} %value_w.1, bf16[16,4096]{1,0:T(8,128)(2,1)} %bitcast.4, f32[1,16]{1,0:T(1,128)} %bitcast.5, f32[1,16]{1,0:T(1,128)} %bitcast.6, ...), custom_call_target="tpu_custom_call" | custom-call | tf_op jit(solution)/shard_map/pallas_call | solution.py:450
  36.8 0.7 %shard_map.96 = (bf16[1,16,16,128]{3,2,1,0:T(8,128)(2,1)}, f32[1,16,128]{2,1,0:T(8,128)}) custom-call(bf16[1,16,16,128]{3,2,1,0:T(8,128)(2,1)S(1)} %get-tuple-element.4.state, f32[1,16,128]{2,1,0:T(8,128)S(1)} %get-tuple-element.5.read), custom_call_target="tpu_custom_call" | custom-call | tf_op jit(solution)/shard_map/pallas_call | solution.py:500

commit v4 on v3

--- a/solution.py
+++ b/solution.py
@@ -208,8 +208,6 @@
 
     for d in range(1, tp):
         feature_copy(d).start()
-    fetch_step(0, 1, tp)
-    fetch_step(1, 1, tp)
 
     def begin(step):
         fetched(step, 0, 1)
@@ -217,16 +215,19 @@
             for j in range(2):
                 total[index, j] = dot(feat[0], weights[index, 0, j])
 
+    fetch_step(0, 1, tp)
+    begin(0)
+    fetch_step(1, 1, tp)
+    begin(1)
     for copy in small:
         copy.wait()
-    before = dot(feat[0], beta_buf[0], ((1,), (1,)))
-    begin(0)
-    begin(1)
+    fetched(0, 1, tp)
+    fetched(1, 1, tp)
     if steps > 2:
         fetch_step(2, 0, tp)
-    fetched(0, 1, tp)
     for d in range(1, tp):
         feature_copy(tp - d).wait_recv()
+    before = dot(feat[0], beta_buf[0], ((1,), (1,)))
     for d in range(1, tp):
         before += dot(feat[d], beta_buf[d], ((1,), (1,)))
     strength_buf[...] = jax.nn.sigmoid(before + bias_buf[...])
@@ -259,6 +260,8 @@
             keep, j = sequence[index]
             if not keep:
                 pair_copy(index, j).start()
+
+    def join(step):
         for index in plan[step]:
             keep, j = sequence[index]
             if keep:
@@ -298,12 +301,22 @@
         if step + 1 < steps:
             skip = 1 if step == 0 else 0
             units = len(plan[step + 1]) * 2 * (tp - skip) * (part // chunk)
-            fetched(step + 1, skip, tp)
+            if step > 0:
+                fetched(step + 1, skip, tp)
             filler = projection(step + 1)
         done = [0, 0]
+        when = 0
+        if step == 2:
+            when = 0
+        elif step == steps - 1:
+            when = 0
+        if step > 0 and when == 0:
+            join(step - 1)
 
         def tick():
             done[0] += 1
+            if step > 0 and done[0] == when:
+                join(step - 1)
             while done[1] * ticks < done[0] * units:
                 done[1] += 1
                 next(filler, None)
@@ -350,7 +363,7 @@
     for h in range(per):
         row = jnp.sum(jnp.where(which == mine * per + h, unit, 0.0), axis=0, keepdims=True)
         ask_buf[h] = jnp.broadcast_to(row, (dim, dim)).T
-    pass_on(steps - 1)
+    join(steps - 1)
     recv[me // 2] = joined[0]
 
     def finish():

time: 37.8 us -> 37 us (0.979)
  Pallas kernels: 36.8 us -> 36 us
    pallas_call x1, Pallas kernels: 36.1 us -> 35.4 us  [shards(): pl.pallas_call(functools.partial(kernel, n, tp, groups, per, dim), out_sh...]
where the time goes in v4:
time: 37 us; the launch traced here: 36.8 us
  Pallas kernels  36 us (97%)
  between operations  0.8 us (2%)
    pallas_call x1, Pallas kernels, shards(): pl.pallas_call(functools.partial(kernel, n, tp, groups, per, dim), out_sh...  35.4 us

profile of v4, /device:TPU:0, one launch (start us, length us, event | category | flops | bytes accessed | tf_op | source)
XLA Modules:
  0.0 36.8 jit_solution(10927219645796793044)
XLA Ops:
  0.6 35.4 %shard_map.95 = (bf16[1,16,16,128]{3,2,1,0:T(8,128)(2,1)S(1)}, f32[1,16,128]{2,1,0:T(8,128)S(1)}) custom-call(bf16[1,256,2048]{2,1,0:T(8,128)(2,1)} %prompt.1, bf16[4096,2048]{1,0:T(8,128)(2,1)} %key_w.1, bf16[4096,2048]{1,0:T(8,128)(2,1)} %value_w.1, bf16[16,4096]{1,0:T(8,128)(2,1)} %bitcast.4, f32[1,16]{1,0:T(1,128)} %bitcast.5, f32[1,16]{1,0:T(1,128)} %bitcast.6, ...), custom_call_target="tpu_custom_call" | custom-call | tf_op jit(solution)/shard_map/pallas_call | solution.py:463
  36.0 0.7 %shard_map.96 = (bf16[1,16,16,128]{3,2,1,0:T(8,128)(2,1)}, f32[1,16,128]{2,1,0:T(8,128)}) custom-call(bf16[1,16,16,128]{3,2,1,0:T(8,128)(2,1)S(1)} %get-tuple-element.4.state, f32[1,16,128]{2,1,0:T(8,128)S(1)} %get-tuple-element.5.read), custom_call_target="tpu_custom_call" | custom-call | tf_op jit(solution)/shard_map/pallas_call | solution.py:513

commit v5 on v4

--- a/solution.py
+++ b/solution.py
@@ -187,6 +187,7 @@
     fetch_step(0, 0, 1)
     fetch_step(1, 0, 1)
 
+    partner_spans[:, :, :, dim:] = jnp.zeros((half, per, dim, dim), BF16)
     barrier = pltpu.get_barrier_semaphore()
     for d in range(1, tp):
         pl.semaphore_signal(barrier, inc=1, device_id={"tp": lax.rem(core + d, tp)}, device_id_type=MESH)
@@ -238,19 +239,23 @@
                 acc += dot(feat[d], weights[index, d, j])
             projected[index, j] = acc.astype(BF16)
 
-    def pair_copy(index, j):
+    def pair_copy(index, j, last=2 * dim):
         return pltpu.make_async_remote_copy(
-            src_ref=spans.at[index], dst_ref=partner_spans.at[j],
+            src_ref=spans.at[index, :, :, :last], dst_ref=partner_spans.at[j, :, :, :last],
             send_sem=pair_send, recv_sem=pair_recv.at[j],
             device_id={"sp": me + 1 - 2 * parity}, device_id_type=MESH,
         )
 
-    def map_copy(j, slot):
+    def map_copy(j, slot, last=2 * dim):
         return pltpu.make_async_remote_copy(
-            src_ref=joined.at[j], dst_ref=recv.at[slot],
+            src_ref=joined.at[j, :, :, :last], dst_ref=recv.at[slot, :, :, :last],
             send_sem=map_send, recv_sem=map_recv.at[slot],
             device_id={"sp": owner(2 * pair_at(j) + parity)}, device_id_type=MESH,
         )
+
+    def by(short, work):
+        pl.when(short)(lambda: work(dim))
+        pl.when(jnp.logical_not(short))(lambda: work(2 * dim))
 
     def is_away(j):
         return owner(2 * pair_at(j) + parity) != me
@@ -259,13 +264,13 @@
         for index in plan[step]:
             keep, j = sequence[index]
             if not keep:
-                pair_copy(index, j).start()
+                by(me == 0, lambda last: pair_copy(index, j, last).start())
 
     def join(step):
         for index in plan[step]:
             keep, j = sequence[index]
             if keep:
-                pair_copy(index, j).wait_recv()
+                by(me == 1, lambda last: pair_copy(index, j, last).wait_recv())
                 for h in range(per):
                     ours, theirs = spans[index, h], partner_spans[j, h]
                     early = jnp.where(parity == 1, theirs, ours)
@@ -275,7 +280,7 @@
                 if j or stride > 1:
                     @pl.when(is_away(j))
                     def _():
-                        map_copy(j, me // 2).start()
+                        by(me < 2, lambda last: map_copy(j, me // 2, last).start())
 
     def projection(step):
         for index in plan[step]:
@@ -370,7 +375,7 @@
         def arrive(p):
             @pl.when(p != me // 2)
             def _():
-                map_copy(0, p).wait_recv()
+                map_copy(0, p, 2 * dim if p else dim).wait_recv()
 
         arrive(0)
         states = [recv[0, h, :, :dim].astype(F32) for h in range(per)]
@@ -410,8 +415,11 @@
 
     def wait_maps(low):
         if low < half:
-            done = joined.at[low:]
-            pltpu.make_async_copy(done, done, map_send).wait()
+            def wait(last):
+                done = joined.at[low:, :, :, :last]
+                pltpu.make_async_copy(done, done, map_send).wait()
+
+            by(me < 2, wait)
 
     if stride == 1:
         wait_all(groups - 1)
@@ -422,7 +430,11 @@
         read_out[0, g * per:(g + 1) * per] = read_recv[g]
     for d in range(1, tp):
         feature_copy(d).wait_send()
-    pltpu.make_async_copy(partner_spans, partner_spans, pair_send).wait()
+    def wait_pairs(last):
+        done = partner_spans.at[:, :, :, :last]
+        pltpu.make_async_copy(done, done, pair_send).wait()
+
+    by(me == 0, wait_pairs)
     if stride == 1:
         wait_maps(1)
     else:

time: 37 us -> 36.7 us (level)
  no operation moved by 1% of the time
where the time goes in v5:
time: 36.7 us; the launch traced here: 36.5 us
  Pallas kernels  35.7 us (97%)
  between operations  0.8 us (2%)
    pallas_call x1, Pallas kernels, shards(): pl.pallas_call(functools.partial(kernel, n, tp, groups, per, dim), out_sh...  35.1 us

profile of v5, /device:TPU:0, one launch (start us, length us, event | category | flops | bytes accessed | tf_op | source)
XLA Modules:
  0.0 36.5 jit_solution(17398957273960292726)
XLA Ops:
  0.6 35.1 %shard_map.95 = (bf16[1,16,16,128]{3,2,1,0:T(8,128)(2,1)S(1)}, f32[1,16,128]{2,1,0:T(8,128)S(1)}) custom-call(bf16[1,256,2048]{2,1,0:T(8,128)(2,1)} %prompt.1, bf16[4096,2048]{1,0:T(8,128)(2,1)} %key_w.1, bf16[4096,2048]{1,0:T(8,128)(2,1)} %value_w.1, bf16[16,4096]{1,0:T(8,128)(2,1)} %bitcast.4, f32[1,16]{1,0:T(1,128)} %bitcast.5, f32[1,16]{1,0:T(1,128)} %bitcast.6, ...), custom_call_target="tpu_custom_call" | custom-call | tf_op jit(solution)/shard_map/pallas_call | solution.py:475
  35.7 0.7 %shard_map.96 = (bf16[1,16,16,128]{3,2,1,0:T(8,128)(2,1)}, f32[1,16,128]{2,1,0:T(8,128)}) custom-call(bf16[1,16,16,128]{3,2,1,0:T(8,128)(2,1)S(1)} %get-tuple-element.4.state, f32[1,16,128]{2,1,0:T(8,128)S(1)} %get-tuple-element.5.read), custom_call_target="tpu_custom_call" | custom-call | tf_op jit(solution)/shard_map/pallas_call | solution.py:525

commit v6 on v5

--- a/solution.py
+++ b/solution.py
@@ -385,7 +385,8 @@
                 write, drop = recv[p, h, :, :dim].astype(F32), recv[p, h, :, dim:]
                 high = states[h].astype(BF16)
                 low = (states[h] - high.astype(F32)).astype(BF16)
-                states[h] = states[h] + (write - dot(drop, high) - dot(drop, low))
+                both = dot(jnp.concatenate([drop, drop], axis=1), under(high, low))
+                states[h] = states[h] + (write - both)
         for h in range(per):
             cast = states[h].astype(BF16)
             for q in range(n):

time: 36.7 us -> 36.7 us (level)
  no operation moved by 1% of the time
where the time goes in v6:
time: 36.7 us; the launch traced here: 36.5 us
  Pallas kernels  35.7 us (97%)
  between operations  0.8 us (2%)
    pallas_call x1, Pallas kernels, shards(): pl.pallas_call(functools.partial(kernel, n, tp, groups, per, dim), out_sh...  35 us

profile of v6, /device:TPU:0, one launch (start us, length us, event | category | flops | bytes accessed | tf_op | source)
XLA Modules:
  0.0 36.5 jit_solution(14845771273112257482)
XLA Ops:
  0.6 35.0 %shard_map.95 = (bf16[1,16,16,128]{3,2,1,0:T(8,128)(2,1)S(1)}, f32[1,16,128]{2,1,0:T(8,128)S(1)}) custom-call(bf16[1,256,2048]{2,1,0:T(8,128)(2,1)} %prompt.1, bf16[4096,2048]{1,0:T(8,128)(2,1)} %key_w.1, bf16[4096,2048]{1,0:T(8,128)(2,1)} %value_w.1, bf16[16,4096]{1,0:T(8,128)(2,1)} %bitcast.4, f32[1,16]{1,0:T(1,128)} %bitcast.5, f32[1,16]{1,0:T(1,128)} %bitcast.6, ...), custom_call_target="tpu_custom_call" | custom-call | tf_op jit(solution)/shard_map/pallas_call | solution.py:476
  35.7 0.7 %shard_map.96 = (bf16[1,16,16,128]{3,2,1,0:T(8,128)(2,1)}, f32[1,16,128]{2,1,0:T(8,128)}) custom-call(bf16[1,16,16,128]{3,2,1,0:T(8,128)(2,1)S(1)} %get-tuple-element.4.state, f32[1,16,128]{2,1,0:T(8,128)S(1)} %get-tuple-element.5.read), custom_call_target="tpu_custom_call" | custom-call | tf_op jit(solution)/shard_map/pallas_call | solution.py:526
